TPU v7x, 32 devices: a whole 2x2x4 slice. The times are simulated.
32 devices in a mesh: sp: 16 (over z, y, x), tp: 2 (over core).
Axes of the slice: x: 2, y: 2, z: 4, core: 2. Of those that a mesh axis runs over, the one named last changes fastest.
Arguments:
- tokens: bfloat16 [2, 4096, 2048], P(None, 'sp'), may hold values from -6 to 6
- key_weight: bfloat16 [2048, 2048], P(None, 'tp'), may hold values from -0.125 to 0.125
- value_weight: bfloat16 [2048, 2048], P(None, 'tp'), may hold values from -0.125 to 0.125
- cum_gate: float32 [2, 4096, 32], P(None, 'sp', 'tp'), may hold values from -493.64 to 0, as said below
- new_input: bfloat16 [2, 2048], replicated, may hold values from -6 to 6
- new_query: bfloat16 [2, 2048], P(None, 'tp'), may hold values from -360 to 360
- new_gate: float32 [2, 32], P(None, 'tp'), may hold values from -493.64 to 0
- out_weight: bfloat16 [2048, 2048], P('tp', 'sp'), may hold values from -0.75 to 0.75
Outputs:
- key_cache: bfloat16 [2, 16, 256, 2048], P(None, 'sp', None, 'tp')
- value_cache: bfloat16 [2, 16, 256, 2048], P(None, 'sp', None, 'tp')
- gate_cache: float32 [2, 16, 256, 32], P(None, 'sp', None, 'tp')
- mixed: bfloat16 [2, 2048], P(None, 'sp')
Inputs may be any that keep to these rules, and one draw needn't show every extreme that they name: For each sequence and head cum_gate does not rise along positions, and new_gate lies at or below the value at the last cached position.
All inputs are finite; a program needn't handle non-finite values.
Results may differ from a plain program's by a relative error of at most 0.015.
Values may be sent and summed in bfloat16 or wider, within the bound.
A program may use at most 64 MiB of HBM per device.

v0:
```python
import jax
import jax.numpy as jnp
from jax import lax
from jax.sharding import PartitionSpec as P


def joined(value, axis, join):
    pieces = jax.tree.map(lambda part: lax.all_gather(part, axis), value)
    head = jax.tree.map(lambda part: part[0], pieces)
    tail = jax.tree.map(lambda part: part[1:], pieces)
    running, _ = lax.scan(lambda running, share: (join(running, share), None), head, tail)
    return running


def combine_parts(first, second):
    highest = jnp.maximum(first[0], second[0])
    first_scale = jnp.exp(first[0] - highest)
    second_scale = jnp.exp(second[0] - highest)
    total = first[1] * first_scale + second[1] * second_scale
    numer = first[2] * first_scale[:, :, None] + second[2] * second_scale[:, :, None]
    return (highest, total, numer)


def body(tokens, key_weight, value_weight, cum_gate, new_input, new_query, new_gate, out_weight):
    local_width = key_weight.shape[1]
    parts = lax.axis_size("sp")
    seq_count, span, width = tokens.shape
    per_peer = span // parts
    flat_rows = tokens.reshape(seq_count * span, width)
    key_local = jnp.dot(flat_rows, key_weight, preferred_element_type=jnp.float32).astype(
        jnp.bfloat16
    )
    value_local = jnp.dot(flat_rows, value_weight, preferred_element_type=jnp.float32).astype(
        jnp.bfloat16
    )
    shaped = (seq_count, per_peer, parts, local_width)
    key_moved, value_moved = (
        lax.all_to_all(key_local.reshape(shaped), "sp", split_axis=2, concat_axis=1, tiled=True),
        lax.all_to_all(value_local.reshape(shaped), "sp", split_axis=2, concat_axis=1, tiled=True),
    )
    key_cache = key_moved.reshape(seq_count, 1, span, local_width)
    value_cache = value_moved.reshape(seq_count, 1, span, local_width)
    head_count = cum_gate.shape[2]
    gate_shaped = cum_gate.reshape(seq_count, per_peer, parts, head_count)
    gate_cache = lax.all_to_all(gate_shaped, "sp", split_axis=2, concat_axis=1, tiled=True).reshape(
        seq_count, 1, span, head_count
    )
    head_size = local_width // head_count
    score_scale = head_size ** (-0.5)
    key_now = jnp.dot(new_input, key_weight, preferred_element_type=jnp.float32).astype(
        jnp.bfloat16
    )
    value_now = jnp.dot(new_input, value_weight, preferred_element_type=jnp.float32).astype(
        jnp.bfloat16
    )
    key_now = key_now.reshape(seq_count, head_count, head_size)
    value_now = value_now.reshape(seq_count, head_count, head_size)
    query_heads = new_query.reshape(seq_count, head_count, head_size)
    key_heads = key_cache.reshape(seq_count, span, head_count, head_size)
    value_heads = value_cache.reshape(seq_count, span, head_count, head_size)
    scores = (
        jnp.einsum("nhd,nlhd->nhl", query_heads, key_heads, preferred_element_type=jnp.float32)
        * score_scale
    )
    scores = (
        scores
        + new_gate[:, :, None]
        - jnp.swapaxes(gate_cache.reshape(seq_count, span, head_count), 1, 2)
    )
    class_top = jnp.max(scores, axis=2)
    expo = jnp.exp(scores - class_top[:, :, None])
    class_total = jnp.sum(expo, axis=2)
    class_num = jnp.einsum(
        "nhl,nlhd->nhd", expo.astype(jnp.bfloat16), value_heads, preferred_element_type=jnp.float32
    )
    cached_top, cached_total, cached_num = joined(
        (class_top, class_total, class_num), "sp", combine_parts
    )
    own_score = (
        jnp.einsum("nhd,nhd->nh", query_heads, key_now, preferred_element_type=jnp.float32)
        * score_scale
    )
    highest = jnp.maximum(cached_top, own_score)
    keep = jnp.exp(cached_top - highest)
    own_expo = jnp.exp(own_score - highest)
    totals = cached_total * keep + own_expo
    own_rounded = lax.optimization_barrier(own_expo.astype(jnp.bfloat16)).astype(jnp.float32)
    numerator = cached_num * keep[:, :, None] + own_rounded[:, :, None] * value_now.astype(
        jnp.float32
    )
    attended = (numerator / totals[:, :, None]).astype(jnp.bfloat16).reshape(seq_count, local_width)
    partial_value = jnp.dot(attended, out_weight, preferred_element_type=jnp.float32)
    partial_value = lax.optimization_barrier(partial_value.astype(jnp.bfloat16)).astype(jnp.float32)
    mixed = lax.psum(partial_value.astype(jnp.bfloat16), "tp")
    return (key_cache, value_cache, gate_cache, mixed)


def solution(mesh):
    placed = (
        P(None, "sp", None),
        P(None, "tp"),
        P(None, "tp"),
        P(None, "sp", "tp"),
        P(),
        P(None, "tp"),
        P(None, "tp"),
        P("tp", "sp"),
    )
    return jax.shard_map(
        body,
        mesh=mesh,
        in_specs=placed,
        out_specs=(
            P(None, "sp", None, "tp"),
            P(None, "sp", None, "tp"),
            P(None, "sp", None, "tp"),
            P(None, "sp"),
        ),
        check_vma=False,
    )
```

profile of v0, /device:TPU:0, one launch (start us, length us, event | category | flops | bytes accessed | tf_op | source)
XLA Modules:
  0.0 194.8 jit_solution(18066433579838654126)
XLA Ops:
  0.6 1.0 reshape.59
  1.9 0.8 reshape.95
  2.7 8.3 %all-to-all-start.2 = ((f32[16,1,512]{2,1,0:T(1,128)}), f32[16,1,512]{2,1,0:T(1,128)S(1)}, u32[]{:S(2)}, u32[]{:S(2)}) async-start(f32[16,1,512]{2,1,0:T(1,128)} %reshape.95), calls=%async_computation.2 | async-start | bytes 65536 | tf_op jit(solution)/shard_map/all_to_all | solution.py:45
  11.1 4.5 %convolution_convert_fusion.1 = bf16[512,1024]{1,0:T(8,128)(2,1)S(1)} fusion(bf16[512,2048]{1,0:T(8,128)(2,1)S(1)} %bitcast.98, bf16[2048,1024]{1,0:T(8,128)(2,1)} %param.11), kind=kOutput, calls=%fused_computation.14 | convolution fusion | flops 2148007936 | bytes 7340032 | tf_op jit(solution)/shard_map/dot_general | solution.py:30
  15.6 1.5 copy.22
  17.1 1.3 all-to-all-done.2
  18.5 5.6 %all-to-all-start = ((bf16[2,16,16,1024]{3,1,0,2:T(8,128)(2,1)}), bf16[2,16,16,1024]{3,1,0,2:T(8,128)(2,1)S(1)}, u32[]{:S(2)}, u32[]{:S(2)}) async-start(bf16[2,16,16,1024]{3,1,0,2:T(8,128)(2,1)} %copy.22), calls=%async_computation | async-start | bytes 2097152 | tf_op jit(solution)/shard_map/all_to_all | solution.py:38
  24.1 4.5 %convolution_convert_fusion = bf16[512,1024]{1,0:T(8,128)(2,1)S(1)} fusion(bf16[512,2048]{1,0:T(8,128)(2,1)S(1)} %bitcast.99, bf16[2048,1024]{1,0:T(8,128)(2,1)} %param.12), kind=kOutput, calls=%fused_computation.13 | convolution fusion | flops 2148007936 | bytes 7340032 | tf_op jit(solution)/shard_map/dot_general | solution.py:33
  28.6 1.6 copy.24
  30.2 17.7 %all-to-all-done = bf16[2,16,16,1024]{3,1,0,2:T(8,128)(2,1)S(1)} async-done(((bf16[2,16,16,1024]{3,1,0,2:T(8,128)(2,1)}), bf16[2,16,16,1024]{3,1,0,2:T(8,128)(2,1)S(1)}, u32[]{:S(2)}, u32[]{:S(2)}) %all-to-all-start) | async-done | bytes 1048608 | tf_op jit(solution)/shard_map/all_to_all | solution.py:38
  47.8 6.0 %all-to-all-start.1 = ((bf16[2,16,16,1024]{3,1,0,2:T(8,128)(2,1)}), bf16[2,16,16,1024]{3,1,0,2:T(8,128)(2,1)}, u32[]{:S(2)}, u32[]{:S(2)}) async-start(bf16[2,16,16,1024]{3,1,0,2:T(8,128)(2,1)} %copy.24), calls=%async_computation.1 | async-start | bytes 2097152 | tf_op jit(solution)/shard_map/all_to_all | solution.py:39
  53.8 2.8 %fusion.7 = f32[2,1024]{1,0:T(2,128)S(1)} fusion(bf16[2,2048]{1,0:T(2,128)(2,1)S(1)} %copy-done.7, bf16[2048,1024]{1,0:T(8,128)(2,1)} %param.12), kind=kOutput, calls=%fused_computation.16 | convolution fusion | flops 8392704 | bytes 4210688 | tf_op jit(solution)/shard_map/dot_general | solution.py:53
  56.9 2.8 %convolution_convert_fusion.3 = bf16[2,1024]{1,0:T(2,128)(2,1)S(1)} fusion(bf16[2,2048]{1,0:T(2,128)(2,1)S(1)} %copy-done.7, bf16[2048,1024]{1,0:T(8,128)(2,1)} %param.11), kind=kOutput, calls=%fused_computation.17 | convolution fusion | flops 8390656 | bytes 4206592 | tf_op jit(solution)/shard_map/dot_general | solution.py:50
  62.4 1.3 copy.55
  63.8 2.3 %reshape_reshape.9 = bf16[2,256,16,64]{3,2,1,0:T(8,128)(2,1)} reshape(bf16[2,16,16,1,1024]{4,2,1,0,3:T(8,128)(2,1)S(1)} %bitcast.100) | data formatting | bytes 2097152 | tf_op jit(solution)/shard_map/reshape;reshape | solution.py:59
  66.1 2.2 %fusion.5 = f32[2,16,1,256]{3,2,1,0:T(1,128)S(1)} fusion(bf16[2,16,64,1]{2,3,1,0:T(2,128)(2,1)S(1)} %reshape.94, bf16[2,256,16,64]{3,2,1,0:T(8,128)(2,1)} %reshape_reshape.9), kind=kOutput, calls=%fused_computation.11 | convolution fusion | flops 1048576 | bytes 1085440 | tf_op jit(solution)/shard_map/nhd,nlhd->nhl/dot_general | solution.py:62
  68.5 41.0 %all-gather.3 = f32[16,2,16]{2,1,0:T(2,128)S(1)} all-gather(f32[1,2,16]{2,1,0:T(2,128)S(1)} %bitcast.110), channel_id=2, replica_groups=mesh['sp'=16,'tp'=2] {'sp'}, dimensions={0}, use_global_device_ids=true | all-gather | bytes 2176 | tf_op jit(solution)/shard_map/all_gather | solution.py:8
  109.7 35.5 %all-gather.4 = f32[16,2,16]{2,1,0:T(2,128)S(1)} all-gather(f32[1,2,16]{2,1,0:T(2,128)S(1)} %bitcast.111), channel_id=3, replica_groups=mesh['sp'=16,'tp'=2] {'sp'}, dimensions={0}, use_global_device_ids=true | all-gather | bytes 2176 | tf_op jit(solution)/shard_map/all_gather | solution.py:8
  145.2 1.3 copy.54
  146.6 2.3 %reshape_reshape.11 = bf16[2,256,16,64]{3,2,1,0:T(8,128)(2,1)} reshape(bf16[2,16,16,1,1024]{4,2,1,0,3:T(8,128)(2,1)S(1)} %bitcast.102) | data formatting | bytes 2097152 | tf_op jit(solution)/shard_map/reshape;reshape | solution.py:60
  148.9 2.1 %fusion.3 = f32[2,16,1,64]{3,2,1,0:T(1,128)S(1)} fusion(bf16[2,256,16,64]{3,2,1,0:T(8,128)(2,1)} %reshape_reshape.11, bf16[2,16,256,1]{2,1,0,3:T(8,128)(2,1)S(1)} %get-tuple-element.76), kind=kOutput, calls=%fused_computation.9 | convolution fusion | flops 1048576 | bytes 1073152 | tf_op jit(solution)/shard_map/nhl,nlhd->nhd/dot_general | solution.py:73
  151.1 38.8 %all-gather.2 = f32[32,16,64]{2,1,0:T(8,128)S(1)} all-gather(f32[2,16,64]{2,1,0:T(8,128)S(1)} %bitcast.109), channel_id=4, replica_groups=mesh['sp'=16,'tp'=2] {'sp'}, dimensions={0}, use_global_device_ids=true | all-gather | bytes 139264 | tf_op jit(solution)/shard_map/all_gather | solution.py:8
  189.9 1.5 while.14
  191.8 3.0 %psum.7 = bf16[2,128]{1,0:T(2,128)(2,1)} all-reduce(bf16[2,128]{1,0:T(2,128)(2,1)S(1)} %convolution_convert_fusion.4), channel_id=1, replica_groups=mesh['sp'=16,'tp'=2] {'tp'}, use_global_device_ids=true, to_apply=%region_4.5 | all-reduce | flops 256 | bytes 1024 | tf_op jit(solution)/shard_map/psum | solution.py:94
  (79 shorter events, 5.4 us)
Async XLA Ops:
  0.6 10.4 %copy-start = (bf16[2,256,2048]{2,1,0:T(8,128)(2,1)S(1)}, bf16[2,256,2048]{2,1,0:T(8,128)(2,1)}, u32[]{:S(2)}) copy-start(bf16[2,256,2048]{2,1,0:T(8,128)(2,1)} %param.10) | copy-start | bytes 6291460
  2.7 15.8 %all-to-all-start.2 = ((f32[16,1,512]{2,1,0:T(1,128)}), f32[16,1,512]{2,1,0:T(1,128)S(1)}, u32[]{:S(2)}, u32[]{:S(2)}) async-start(f32[16,1,512]{2,1,0:T(1,128)} %reshape.95), calls=%async_computation.2 | async-start | bytes 65536 | tf_op jit(solution)/shard_map/all_to_all | solution.py:45
  18.5 29.4 %all-to-all-start = ((bf16[2,16,16,1024]{3,1,0,2:T(8,128)(2,1)}), bf16[2,16,16,1024]{3,1,0,2:T(8,128)(2,1)S(1)}, u32[]{:S(2)}, u32[]{:S(2)}) async-start(bf16[2,16,16,1024]{3,1,0,2:T(8,128)(2,1)} %copy.22), calls=%async_computation | async-start | bytes 2097152 | tf_op jit(solution)/shard_map/all_to_all | solution.py:38
  28.6 25.2 %copy-start.7 = (bf16[2,2048]{1,0:T(2,128)(2,1)S(1)}, bf16[2,2048]{1,0:T(2,128)(2,1)}, u32[]{:S(2)}) copy-start(bf16[2,2048]{1,0:T(2,128)(2,1)} %param.14) | copy-start | bytes 24580
  47.8 8.8 %copy-start.3 = (bf16[2,16,16,1024]{3,1,0,2:T(8,128)(2,1)}, bf16[2,16,16,1024]{3,1,0,2:T(8,128)(2,1)S(1)}, u32[]{:S(2)}) copy-start(bf16[2,16,16,1024]{3,1,0,2:T(8,128)(2,1)S(1)} %all-to-all-done) | copy-start | bytes 3145732
  47.8 97.4 %all-to-all-start.1 = ((bf16[2,16,16,1024]{3,1,0,2:T(8,128)(2,1)}), bf16[2,16,16,1024]{3,1,0,2:T(8,128)(2,1)}, u32[]{:S(2)}, u32[]{:S(2)}) async-start(bf16[2,16,16,1024]{3,1,0,2:T(8,128)(2,1)} %copy.24), calls=%async_computation.1 | async-start | bytes 2097152 | tf_op jit(solution)/shard_map/all_to_all | solution.py:39
  53.8 2.9 %copy-start.8 = (bf16[2,1024]{1,0:T(2,128)(2,1)S(1)}, bf16[2,1024]{1,0:T(2,128)(2,1)}, u32[]{:S(2)}) copy-start(bf16[2,1024]{1,0:T(2,128)(2,1)} %param.15) | copy-start | bytes 12292
  63.8 4.6 %copy-start.1 = (bf16[2,16,16,1024]{3,1,2,0:T(8,128)(2,1)}, bf16[2,16,16,1024]{3,1,2,0:T(8,128)(2,1)S(1)}, u32[]{:S(2)}) copy-start(bf16[2,16,16,1024]{3,1,2,0:T(8,128)(2,1)S(1)} %copy.55) | copy-start | bytes 3145732
  66.1 2.3 %copy-start.9 = (f32[2,16]{1,0:T(2,128)S(1)}, f32[2,16]{1,0:T(2,128)}, u32[]{:S(2)}) copy-start(f32[2,16]{1,0:T(2,128)} %param.16) | copy-start | bytes 388
  109.5 39.4 %copy-start.5 = (f32[16,2,16]{2,1,0:T(2,128)}, f32[16,2,16]{2,1,0:T(2,128)S(1)}, u32[]{:S(2)}) copy-start(f32[16,2,16]{2,1,0:T(2,128)S(1)} %all-gather.3) | copy-start | bytes 6148
  145.2 3.7 %copy-start.6 = (f32[16,2,16]{2,1,0:T(2,128)}, f32[16,2,16]{2,1,0:T(2,128)S(1)}, u32[]{:S(2)}) copy-start(f32[16,2,16]{2,1,0:T(2,128)S(1)} %all-gather.4) | copy-start | bytes 6148
  146.5 4.5 %copy-start.2 = (bf16[2,16,16,1024]{3,1,2,0:T(8,128)(2,1)}, bf16[2,16,16,1024]{3,1,2,0:T(8,128)(2,1)S(1)}, u32[]{:S(2)}) copy-start(bf16[2,16,16,1024]{3,1,2,0:T(8,128)(2,1)S(1)} %copy.54) | copy-start | bytes 3145732
  148.9 42.8 %copy-start.4 = (bf16[1024,128]{1,0:T(8,128)(2,1)S(1)}, bf16[1024,128]{1,0:T(8,128)(2,1)}, u32[]{:S(2)}) copy-start(bf16[1024,128]{1,0:T(8,128)(2,1)} %param.17) | copy-start | bytes 786436
  148.9 41.0 %slice-start = ((f32[16,2,16]{2,1,0:T(2,128)}), f32[15,2,16]{2,1,0:T(2,128)S(1)}, s32[]{:S(2)}) async-start(f32[16,2,16]{2,1,0:T(2,128)} %copy-done.5), calls=%async_computation.3 | async-start | bytes 30720 | tf_op jit(solution)/shard_map/slice | solution.py:10
  148.9 41.0 %slice-start.1 = ((f32[16,2,16]{2,1,0:T(2,128)}), f32[15,2,16]{2,1,0:T(2,128)S(1)}, s32[]{:S(2)}) async-start(f32[16,2,16]{2,1,0:T(2,128)} %copy-done.6), calls=%async_computation.4 | async-start | bytes 30720 | tf_op jit(solution)/shard_map/slice | solution.py:10
where the time goes:
time: 195 us
  blocking collectives  118 us (61%)
  starting transfers between devices  19.9 us (10%)
  matrix products  19.3 us (10%)
  waiting for transfers between devices  19 us (10%)
  local copies, waits for them, and re-layouts  14.7 us (8%)
  other arithmetic  2.71 us (1%)
    all_gather x3, blocking collectives, joined(): pieces = jax.tree.map(lambda part: lax.all_gather(part, axis), value)  115 us
    all_to_all x1, waiting for transfers between devices, body(): lax.all_to_all(key_local.reshape(shaped), 'sp', split_axis=2, concat_axis...  17.7 us
    all_to_all x1, starting transfers between devices, body(): lax.all_to_all(gate_shaped, 'sp', split_axis=2, concat_axis=1, tiled=True)  8.34 us
    all_to_all x1, starting transfers between devices, body(): lax.all_to_all(value_local.reshape(shaped), 'sp', split_axis=2, concat_ax...  5.96 us
    all_to_all x1, starting transfers between devices, body(): lax.all_to_all(key_local.reshape(shaped), 'sp', split_axis=2, concat_axis...  5.59 us
    dot_general x1, matrix products, body(): jnp.dot(flat_rows, key_weight, preferred_element_type=jnp.float32)  4.52 us
    dot_general x1, matrix products, body(): jnp.dot(flat_rows, value_weight, preferred_element_type=jnp.float32)  4.52 us
  transfers between devices with their start and end apart: 3, of which 2 were waited for; matrix products, arithmetic and copies ran while one was open for 14% of the time, Pallas kernels for 0%

commit v1 on v0

--- a/solution.py
+++ b/solution.py
@@ -1,7 +1,17 @@
+import functools
 import jax
 import jax.numpy as jnp
 from jax import lax
+from jax.experimental import pallas as pl
+from jax.experimental.pallas import tpu as pltpu
 from jax.sharding import PartitionSpec as P
+
+MESH = pl.DeviceIdType.MESH
+F32 = jnp.float32
+BF16 = jnp.bfloat16
+EXACT = lax.Precision.HIGHEST
+GROUPS = 4
+TILE = 256
 
 
 def joined(value, axis, join):
@@ -21,7 +31,7 @@
     return (highest, total, numer)
 
 
-def body(tokens, key_weight, value_weight, cum_gate, new_input, new_query, new_gate, out_weight):
+def plain_body(tokens, key_weight, value_weight, cum_gate, new_input, new_query, new_gate, out_weight):
     local_width = key_weight.shape[1]
     parts = lax.axis_size("sp")
     seq_count, span, width = tokens.shape
@@ -93,6 +103,437 @@
     partial_value = lax.optimization_barrier(partial_value.astype(jnp.bfloat16)).astype(jnp.float32)
     mixed = lax.psum(partial_value.astype(jnp.bfloat16), "tp")
     return (key_cache, value_cache, gate_cache, mixed)
+
+
+def iota(shape, axis):
+    return lax.broadcasted_iota(jnp.int32, shape, axis)
+
+
+def dot(a, b, contract=((1,), (0,)), precision=None):
+    return lax.dot_general(
+        a, b, (contract, ((), ())), precision=precision, preferred_element_type=F32
+    )
+
+
+def one_hot(condition, dtype):
+    return jnp.where(condition, 1.0, 0.0).astype(dtype)
+
+
+def kernel(
+    n, m, heads, head_size,
+    tokens_ref, wk_ref, wv_ref, gate_ref, input_ref, query_ref, newgate_ref, ow_ref,
+    kc_ref, vc_ref, gc_ref, mixed_ref,
+    tok, wk, wv, ow, psend, recv, kst, vst, gsend, grecv, qblk, scores, expo,
+    know, vnow, stat, statall, num, numall, coef, xsend, xrecv,
+    load_sem, own_sem, out_sem, tok_ss, tok_rs, fwd_ss, fwd_rs, gate_ss, gate_rs,
+    stat_ss, stat_rs, num_ss, num_rs, x_ss, x_rs,
+):
+    me = lax.axis_index("sp")
+    t = lax.axis_index("tp")
+    other = 1 - t
+    seqs, span, width = tokens_ref.shape
+    local = wk_ref.shape[1]
+    tiles = local // TILE
+    per_group = n // GROUPS
+    log_m = m.bit_length() - 1
+    log_hd = head_size.bit_length() - 1
+    scale = head_size ** (-0.5)
+
+    loads = [
+        pltpu.make_async_copy(tokens_ref.at[t], tok.at[t], load_sem.at[0]),
+        pltpu.make_async_copy(tokens_ref.at[other], tok.at[other], load_sem.at[1]),
+        pltpu.make_async_copy(wk_ref, wk, load_sem.at[2]),
+        pltpu.make_async_copy(wv_ref, wv, load_sem.at[3]),
+        pltpu.make_async_copy(ow_ref, ow, load_sem.at[4]),
+    ]
+    for load in loads:
+        load.start()
+
+    barrier = pltpu.get_barrier_semaphore()
+
+    def greet(k, carry):
+        pl.semaphore_signal(
+            barrier, inc=1, device_id=(lax.rem(me + k, n), t), device_id_type=MESH
+        )
+        return carry
+
+    lax.fori_loop(1, n, greet, 0)
+    pl.semaphore_signal(barrier, inc=1, device_id=(me, other), device_id_type=MESH)
+
+    quarter = m // 4
+    stacked = jnp.concatenate([gate_ref[...]] * 4, axis=0)
+    row = iota((span, span), 0)
+    col = iota((span, span), 1)
+    block_rows = n * quarter
+    log_q = quarter.bit_length() - 1
+    step_q = row >> (block_rows.bit_length() - 1)
+    inner = row & (block_rows - 1)
+    place = (step_q * quarter + (inner & (quarter - 1))) * n + (inner >> log_q)
+    moved_gate = dot(one_hot(col == place, F32), stacked, ((1,), (1,)), EXACT)
+    lanes = seqs * heads
+    keep_lane = (iota(moved_gate.shape, 1) // lanes) == (
+        iota(moved_gate.shape, 0) >> (block_rows.bit_length() - 1)
+    )
+    moved_gate = jnp.where(keep_lane, moved_gate, 0.0)
+    packed = moved_gate[0:block_rows]
+    for q in range(1, 4):
+        packed = packed + moved_gate[q * block_rows : (q + 1) * block_rows]
+    for r in range(n):
+        gsend[r] = packed[r * quarter : (r + 1) * quarter]
+
+    loads[0].wait()
+    perm = one_hot(col == (row & (m - 1)) * n + (row >> log_m), BF16)
+    for j in range(width // 512):
+        cols = slice(j * 512, (j + 1) * 512)
+        psend[:, :, cols] = dot(perm, tok[t, :, cols]).astype(BF16).reshape(n, m, 512)
+
+    head_of = iota((heads, local), 1) >> log_hd
+    mine = head_of == iota((heads, local), 0)
+    for b in range(seqs):
+        qblk[b * heads : (b + 1) * heads] = jnp.where(
+            mine, query_ref[b : b + 1, :].astype(F32), 0.0
+        ).astype(BF16)
+    scores[...] = jnp.zeros_like(scores)
+
+    pl.semaphore_wait(barrier, n)
+
+    def peer(k):
+        far = lax.div(k, per_group)
+        near = lax.rem(k, per_group)
+        zone = lax.rem(lax.div(me, per_group) + far, GROUPS)
+        return zone * per_group + lax.rem(lax.rem(me, per_group) + near, per_group)
+
+    def tok_copy(k, to, source):
+        return pltpu.make_async_remote_copy(
+            src_ref=psend.at[to], dst_ref=recv.at[t, source],
+            send_sem=tok_ss.at[k], recv_sem=tok_rs.at[source],
+            device_id=(to, t), device_id_type=MESH,
+        )
+
+    def gate_copy(k, to, source):
+        return pltpu.make_async_remote_copy(
+            src_ref=gsend.at[to], dst_ref=grecv.at[source],
+            send_sem=gate_ss.at[k], recv_sem=gate_rs.at[source],
+            device_id=(to, t), device_id_type=MESH,
+        )
+
+    def stat_copy(k, to, source):
+        return pltpu.make_async_remote_copy(
+            src_ref=stat, dst_ref=statall.at[source],
+            send_sem=stat_ss.at[k], recv_sem=stat_rs.at[source],
+            device_id=(to, t), device_id_type=MESH,
+        )
+
+    def num_copy(k, to, source):
+        return pltpu.make_async_remote_copy(
+            src_ref=num, dst_ref=numall.at[source],
+            send_sem=num_ss.at[k], recv_sem=num_rs.at[source],
+            device_id=(to, t), device_id_type=MESH,
+        )
+
+    def forward(held, source, target_batch):
+        return pltpu.make_async_remote_copy(
+            src_ref=held, dst_ref=recv.at[target_batch, source],
+            send_sem=fwd_ss.at[source], recv_sem=fwd_rs.at[source],
+            device_id=(me, other), device_id_type=MESH,
+        )
+
+    def send_tokens(k, carry):
+        tok_copy(k, peer(k), me).start()
+        return carry
+
+    def send_gates(k, carry):
+        gate_copy(k, peer(k), me).start()
+        return carry
+
+    lax.fori_loop(1, n, send_gates, 0)
+    for lo, hi in SEND_ORDER(per_group):
+        lax.fori_loop(lo, hi, send_tokens, 0)
+    own_copy = pltpu.make_async_copy(psend.at[me], recv.at[t, me], own_sem)
+    own_copy.start()
+    forward(psend.at[me], me, t).start()
+
+    loads[1].wait()
+    loads[2].wait()
+
+    def key_tile(j, carry):
+        cols = pl.ds(pl.multiple_of(j * TILE, TILE), TILE)
+        weight = wk[:, cols]
+        know[:, cols] = dot(input_ref[...], weight).astype(BF16).astype(F32)
+        for b in range(seqs):
+            keys = dot(tok[b], weight).astype(BF16)
+            rows = slice(b * heads, (b + 1) * heads)
+            scores[rows] += dot(qblk[rows, cols], keys, ((1,), (1,)))
+        return carry
+
+    lax.fori_loop(0, tiles, key_tile, 0)
+
+    eye = iota((heads, heads), 0) == iota((heads, heads), 1)
+    eye_wide = iota((heads, 128), 0) == iota((heads, 128), 1)
+    for b in range(seqs):
+        rows = slice(b * heads, (b + 1) * heads)
+        lift = jnp.sum(jnp.where(eye, newgate_ref[b : b + 1, :], 0.0), axis=1, keepdims=True)
+        score = scores[rows] * scale + lift - gate_ref[rows]
+        top = jnp.max(score, axis=1, keepdims=True)
+        weights = jnp.exp(score - top)
+        total = jnp.sum(weights, axis=1, keepdims=True)
+        expo[rows] = weights.astype(BF16)
+        stat[b : b + 1, :] = jnp.sum(jnp.where(eye_wide, top, 0.0), axis=0, keepdims=True)
+        stat[seqs + b : seqs + b + 1, :] = jnp.sum(
+            jnp.where(eye_wide, total, 0.0), axis=0, keepdims=True
+        )
+
+    loads[3].wait()
+
+    def value_tile(j, carry):
+        cols = pl.ds(pl.multiple_of(j * TILE, TILE), TILE)
+        weight = wv[:, cols]
+        vnow[:, cols] = dot(input_ref[...], weight).astype(BF16).astype(F32)
+        held = (iota((heads, TILE), 1) >> log_hd) + j * (TILE // head_size)
+        ours = held == iota((heads, TILE), 0)
+        sums = []
+        for b in range(seqs):
+            values = dot(tok[b], weight).astype(BF16)
+            full = dot(expo[b * heads : (b + 1) * heads], values)
+            sums.append(jnp.sum(jnp.where(ours, full, 0.0), axis=0, keepdims=True))
+        num[:, cols] = jnp.concatenate(sums, axis=0).astype(BF16)
+        return carry
+
+    lax.fori_loop(0, tiles, value_tile, 0)
+
+    def send_read(k, carry):
+        stat_copy(k, peer(k), me).start()
+        num_copy(k, peer(k), me).start()
+        return carry
+
+    statall[me] = stat[...]
+    numall[me] = num[...]
+    lax.fori_loop(1, n, send_read, 0)
+
+    def out_copies(zone):
+        rows = pl.ds(pl.multiple_of(zone * per_group * m, per_group * m), per_group * m)
+        return (
+            pltpu.make_async_copy(kst.at[:, rows], kc_ref.at[:, rows], out_sem.at[0, zone]),
+            pltpu.make_async_copy(vst.at[:, rows], vc_ref.at[:, rows], out_sem.at[1, zone]),
+        )
+
+    def pass_on(far, near_from):
+        def step(near, carry):
+            source = peer(far * per_group + near)
+            tok_copy(0, source, source).wait_recv()
+            forward(recv.at[t, source], source, t).start()
+            return carry
+
+        lax.fori_loop(near_from, per_group, step, 0)
+
+    def project(far):
+        zone = lax.rem(lax.div(me, per_group) + far, GROUPS)
+        start = zone * per_group
+
+        def arrived(near, carry):
+            forward(recv.at[other, start + near], start + near, other).wait_recv()
+            return carry
+
+        lax.fori_loop(0, per_group, arrived, 0)
+        rows = pl.ds(pl.multiple_of(start * m, per_group * m), per_group * m)
+
+        def tile(j, carry):
+            cols = pl.ds(pl.multiple_of(j * TILE, TILE), TILE)
+            block = recv[:, pl.ds(start, per_group)].reshape(seqs * per_group * m, width)
+            made = dot(block, wk[:, cols]).astype(BF16)
+            kst[:, rows, cols] = made.reshape(seqs, per_group * m, TILE)
+            made = dot(block, wv[:, cols]).astype(BF16)
+            vst[:, rows, cols] = made.reshape(seqs, per_group * m, TILE)
+            return carry
+
+        lax.fori_loop(0, tiles, tile, 0)
+        for copy in out_copies(zone):
+            copy.start()
+
+    def finish_gates():
+        def arrived(k, carry):
+            source = peer(k)
+            gate_copy(k, source, source).wait_recv()
+            return carry
+
+        lax.fori_loop(1, n, arrived, 0)
+        grecv[me] = gsend[me]
+        held = jnp.concatenate([grecv[s] for s in range(n)], axis=0)
+        place_row = iota((block_rows, span), 0)
+        target = ((place_row >> log_q) << log_m) + (place_row & (quarter - 1))
+        spot = iota((block_rows, span), 1)
+        result = None
+        for q in range(4):
+            part = dot(held, one_hot(spot == target + q * quarter, F32), ((0,), (0,)), EXACT)
+            part = part[q * lanes : (q + 1) * lanes]
+            result = part if result is None else result + part
+        gc_ref[...] = result
+
+    def finish_read():
+        def arrived(k, carry):
+            source = peer(k)
+            stat_copy(k, source, source).wait_recv()
+            num_copy(k, source, source).wait_recv()
+            return carry
+
+        lax.fori_loop(1, n, arrived, 0)
+        loads[4].wait()
+        widen = one_hot((iota((128, local), 1) >> log_hd) == iota((128, local), 0), F32)
+        own = dot(query_ref[...].astype(F32) * know[...], widen, ((1,), (1,)), EXACT) * scale
+        numbers = numall[...].astype(F32)
+        attended = []
+        for b in range(seqs):
+            tops = statall[:, b, :]
+            totals = statall[:, seqs + b, :]
+            cached_top = jnp.max(tops, axis=0, keepdims=True)
+            weight = jnp.exp(tops - cached_top)
+            cached_total = jnp.sum(weight * totals, axis=0, keepdims=True)
+            own_score = own[b : b + 1]
+            highest = jnp.maximum(cached_top, own_score)
+            keep = jnp.exp(cached_top - highest)
+            own_expo = jnp.exp(own_score - highest)
+            total = cached_total * keep + own_expo
+            coef[0:n] = weight * (keep / total)
+            coef[n : n + 8] = jnp.broadcast_to(own_expo.astype(BF16).astype(F32) / total, (8, 128))
+            wide = dot(coef[...], widen, precision=EXACT)
+            cached = jnp.sum(numbers[:, b, :] * wide[0:n], axis=0, keepdims=True)
+            attended.append(cached + vnow[b : b + 1, :] * wide[n : n + 1])
+        attended = jnp.concatenate(attended, axis=0).astype(BF16)
+        xsend[...] = dot(attended, ow[...]).astype(BF16)
+
+    own_copy.wait()
+    pass_on(0, 1)
+    finish_gates()
+    project(0)
+    for far in FAR_ORDER[:-1]:
+        pass_on(far, 0)
+        project(far)
+    finish_read()
+    swap = pltpu.make_async_remote_copy(
+        src_ref=xsend, dst_ref=xrecv, send_sem=x_ss, recv_sem=x_rs,
+        device_id=(me, other), device_id_type=MESH,
+    )
+    swap.start()
+    pass_on(FAR_ORDER[-1], 0)
+    project(FAR_ORDER[-1])
+    swap.wait()
+    mixed_ref[...] = (xsend[...].astype(F32) + xrecv[...].astype(F32)).astype(BF16)
+
+    def sent(k, carry):
+        to = peer(k)
+        tok_copy(k, to, me).wait_send()
+        gate_copy(k, to, me).wait_send()
+        stat_copy(k, to, me).wait_send()
+        num_copy(k, to, me).wait_send()
+        return carry
+
+    lax.fori_loop(1, n, sent, 0)
+
+    def passed(source, carry):
+        forward(recv.at[t, source], source, t).wait_send()
+        return carry
+
+    lax.fori_loop(0, n, passed, 0)
+    for zone in range(GROUPS):
+        for copy in out_copies(zone):
+            copy.wait()
+
+
+FAR_ORDER = (1, 3, 2)
+
+
+def SEND_ORDER(per_group):
+    order = [(far * per_group, (far + 1) * per_group) for far in (2, 1, 3)]
+    return order + [(1, per_group)]
+
+
+def body(tokens, key_weight, value_weight, cum_gate, new_input, new_query, new_gate, out_weight):
+    n = lax.axis_size("sp")
+    seqs, span, width = tokens.shape
+    local = key_weight.shape[1]
+    heads = cum_gate.shape[2]
+    head_size = local // heads
+    m = span // n
+    out_cols = out_weight.shape[1]
+    gates = jnp.swapaxes(cum_gate, 1, 2).reshape(seqs * heads, span)
+    anywhere = pl.BlockSpec(memory_space=pl.ANY)
+    inside = pl.BlockSpec(memory_space=pltpu.VMEM)
+    dma = pltpu.SemaphoreType.DMA
+    key_cache, value_cache, gate_cache, mixed = pl.pallas_call(
+        functools.partial(kernel, n, m, heads, head_size),
+        out_shape=(
+            jax.ShapeDtypeStruct((seqs, span, local), BF16),
+            jax.ShapeDtypeStruct((seqs, span, local), BF16),
+            jax.ShapeDtypeStruct((seqs * heads, span), F32),
+            jax.ShapeDtypeStruct((seqs, out_cols), BF16),
+        ),
+        in_specs=[anywhere, anywhere, anywhere, inside, inside, inside, inside, anywhere],
+        out_specs=(anywhere, anywhere, inside, inside),
+        scratch_shapes=[
+            pltpu.VMEM((seqs, span, width), BF16),
+            pltpu.VMEM((width, local), BF16),
+            pltpu.VMEM((width, local), BF16),
+            pltpu.VMEM(out_weight.shape, BF16),
+            pltpu.VMEM((n, m, width), BF16),
+            pltpu.VMEM((seqs, n, m, width), BF16),
+            pltpu.VMEM((seqs, span, local), BF16),
+            pltpu.VMEM((seqs, span, local), BF16),
+            pltpu.VMEM((n, m // 4, 128), F32),
+            pltpu.VMEM((n, m // 4, 128), F32),
+            pltpu.VMEM((seqs * heads, local), BF16),
+            pltpu.VMEM((seqs * heads, span), F32),
+            pltpu.VMEM((seqs * heads, span), BF16),
+            pltpu.VMEM((seqs, local), F32),
+            pltpu.VMEM((seqs, local), F32),
+            pltpu.VMEM((2 * seqs, 128), F32),
+            pltpu.VMEM((n, 2 * seqs, 128), F32),
+            pltpu.VMEM((seqs, local), BF16),
+            pltpu.VMEM((n, seqs, local), BF16),
+            pltpu.VMEM((n + 8, 128), F32),
+            pltpu.VMEM((seqs, out_cols), BF16),
+            pltpu.VMEM((seqs, out_cols), BF16),
+            dma((5,)),
+            dma,
+            dma((2, GROUPS)),
+        ]
+        + [dma((n,))] * 10
+        + [dma, dma],
+        compiler_params=pltpu.CompilerParams(
+            collective_id=0, has_side_effects=True, vmem_limit_bytes=60 * 1024 * 1024
+        ),
+    )(tokens, key_weight, value_weight, gates, new_input, new_query, new_gate, out_weight)
+    gate_cache = jnp.swapaxes(gate_cache.reshape(seqs, heads, span), 1, 2)
+    return (
+        key_cache[:, None],
+        value_cache[:, None],
+        gate_cache[:, None],
+        mixed,
+    )
+
+
+def fits(mesh):
+    def holds(tokens, key_weight, value_weight, cum_gate, *rest):
+        n = lax.axis_size("sp")
+        seqs, span, width = tokens.shape
+        heads = cum_gate.shape[2]
+        local = key_weight.shape[1]
+        m = span // n
+        return (
+            lax.axis_size("tp") == 2
+            and seqs == 2
+            and m % 16 == 0
+            and m & (m - 1) == 0
+            and n % GROUPS == 0
+            and n & (n - 1) == 0
+            and 4 * seqs * heads == 128
+            and local % TILE == 0
+            and width % 512 == 0
+        )
+
+    def chosen(*arrays):
+        return body(*arrays) if holds(*arrays) else plain_body(*arrays)
+
+    return chosen
 
 
 def solution(mesh):
@@ -107,7 +548,7 @@
         P("tp", "sp"),
     )
     return jax.shard_map(
-        body,
+        fits(mesh),
         mesh=mesh,
         in_specs=placed,
         out_specs=(

time: 195 us -> 52.7 us (0.27)
  the two profiles are of different devices: /device:TPU:0 before, /device:TPU:9 now
where the time goes in v1:
time: 52.7 us; the launch traced here: 52.5 us
  Pallas kernels  46.1 us (87%)
  local copies, waits for them, and re-layouts  5.66 us (11%)
  between operations  0.66 us (1%)
    pallas_call x1, Pallas kernels, body(): pl.pallas_call(functools.partial(kernel, n, m, heads, head_size), out_sha...  46.1 us
    unnamed x8, local copies, waits for them, and re-layouts  5.66 us

profile of v1, /device:TPU:9, one launch (start us, length us, event | category | flops | bytes accessed | tf_op | source)
XLA Modules:
  0.0 52.5 jit_solution(9142935523036668869)
XLA Ops:
  0.6 46.1 %shard_map.111 = (bf16[2,256,1024]{2,1,0:T(8,128)(2,1)}, bf16[2,256,1024]{2,1,0:T(8,128)(2,1)}, f32[32,256]{1,0:T(8,128)}, bf16[2,128]{1,0:T(2,128)(2,1)}) custom-call(bf16[2,256,2048]{2,1,0:T(8,128)(2,1)} %tokens_ref.1, bf16[2048,1024]{1,0:T(8,128)(2,1)} %wk_ref.1, bf16[2048,1024]{1,0:T(8,128)(2,1)} %wv_ref.1, f32[32,256]{1,0:T(8,128)} %bitcast.16, ...), custom_call_target="tpu_custom_call" | custom-call | tf_op jit(solution)/shard_map/pallas_call | solution.py:462
  46.8 0.0 copy-start
  46.8 0.0 copy-start.1
  46.8 2.3 %copy.18 = bf16[2,1,256,1024]{3,2,1,0:T(8,128)(2,1)} copy(bf16[2,1,256,1024]{3,2,1,0:T(8,128)(2,1)} %bitcast.15) | data formatting | bytes 2097152
  49.1 2.3 %copy.19 = bf16[2,1,256,1024]{3,2,1,0:T(8,128)(2,1)} copy(bf16[2,1,256,1024]{3,2,1,0:T(8,128)(2,1)} %bitcast.14) | data formatting | bytes 2097152
  51.3 0.0 copy-done
  51.3 0.6 %copy.20 = f32[2,1,256,16]{2,3,1,0:T(8,128)} copy(f32[2,1,256,16]{2,3,1,0:T(8,128)S(1)} %bitcast.17) | data formatting | bytes 65536
  51.9 0.0 copy-done.1
  52.0 0.5 copy.21
Async XLA Ops:
  46.8 4.5 %copy-start = (f32[32,256]{1,0:T(8,128)S(1)}, f32[32,256]{1,0:T(8,128)}, u32[]{:S(2)}) copy-start(f32[32,256]{1,0:T(8,128)} %get-tuple-element.10) | copy-start | bytes 98308
  46.8 5.2 %copy-start.1 = (bf16[2,128]{1,0:T(2,128)(2,1)S(1)}, bf16[2,128]{1,0:T(2,128)(2,1)}, u32[]{:S(2)}) copy-start(bf16[2,128]{1,0:T(2,128)(2,1)} %get-tuple-element.23) | copy-start | bytes 1540

commit v2 on v1

--- a/solution.py
+++ b/solution.py
@@ -121,11 +121,12 @@
 
 def kernel(
     n, m, heads, head_size,
-    tokens_ref, wk_ref, wv_ref, gate_ref, input_ref, query_ref, newgate_ref, ow_ref,
-    kc_ref, vc_ref, gc_ref, mixed_ref,
-    tok, wk, wv, ow, psend, recv, kst, vst, gsend, grecv, qblk, scores, expo,
+    tokens_ref, wk_ref, wv_ref, gate_in, input_in, query_in, newgate_in, ow_ref,
+    kst, vst, gc_ref, mixed_ref,
+    gate_ref, input_ref, query_ref, newgate_ref,
+    tok, wk, wv, ow, psend, recv, gsend, grecv, qblk, scores, expo,
     know, vnow, stat, statall, num, numall, coef, xsend, xrecv,
-    load_sem, own_sem, out_sem, tok_ss, tok_rs, fwd_ss, fwd_rs, gate_ss, gate_rs,
+    load_sem, own_sem, tok_ss, tok_rs, fwd_ss, fwd_rs, gate_ss, gate_rs,
     stat_ss, stat_rs, num_ss, num_rs, x_ss, x_rs,
 ):
     me = lax.axis_index("sp")
@@ -139,6 +140,12 @@
     log_hd = head_size.bit_length() - 1
     scale = head_size ** (-0.5)
 
+    small = [
+        pltpu.make_async_copy(gate_in, gate_ref, load_sem.at[5]),
+        pltpu.make_async_copy(input_in, input_ref, load_sem.at[6]),
+        pltpu.make_async_copy(query_in, query_ref, load_sem.at[7]),
+        pltpu.make_async_copy(newgate_in, newgate_ref, load_sem.at[8]),
+    ]
     loads = [
         pltpu.make_async_copy(tokens_ref.at[t], tok.at[t], load_sem.at[0]),
         pltpu.make_async_copy(tokens_ref.at[other], tok.at[other], load_sem.at[1]),
@@ -146,8 +153,7 @@
         pltpu.make_async_copy(wv_ref, wv, load_sem.at[3]),
         pltpu.make_async_copy(ow_ref, ow, load_sem.at[4]),
     ]
-    for load in loads:
-        load.start()
+    loads[0].start()
 
     barrier = pltpu.get_barrier_semaphore()
 
@@ -159,6 +165,84 @@
 
     lax.fori_loop(1, n, greet, 0)
     pl.semaphore_signal(barrier, inc=1, device_id=(me, other), device_id_type=MESH)
+
+    loads[0].wait()
+    for load in small + loads[1:]:
+        load.start()
+    row = iota((span, span), 0)
+    col = iota((span, span), 1)
+    perm = one_hot(col == (row & (m - 1)) * n + (row >> log_m), BF16)
+    for j in range(width // 512):
+        cols = slice(j * 512, (j + 1) * 512)
+        psend[:, :, cols] = dot(perm, tok[t, :, cols]).astype(BF16).reshape(n, m, 512)
+
+    for load in small:
+        load.wait()
+    head_of = iota((heads, local), 1) >> log_hd
+    mine = head_of == iota((heads, local), 0)
+    for b in range(seqs):
+        qblk[b * heads : (b + 1) * heads] = jnp.where(
+            mine, query_ref[b : b + 1, :].astype(F32), 0.0
+        ).astype(BF16)
+    scores[...] = jnp.zeros_like(scores)
+
+    pl.semaphore_wait(barrier, n)
+
+    def peer(k):
+        far = lax.div(k, per_group)
+        near = lax.rem(k, per_group)
+        zone = lax.rem(lax.div(me, per_group) + far, GROUPS)
+        return zone * per_group + lax.rem(lax.rem(me, per_group) + near, per_group)
+
+    def tok_copy(k, to, source):
+        return pltpu.make_async_remote_copy(
+            src_ref=psend.at[to], dst_ref=recv.at[t, source],
+            send_sem=tok_ss.at[k], recv_sem=tok_rs.at[source],
+            device_id=(to, t), device_id_type=MESH,
+        )
+
+    def gate_copy(k, to, source):
+        return pltpu.make_async_remote_copy(
+            src_ref=gsend.at[to], dst_ref=grecv.at[source],
+            send_sem=gate_ss.at[k], recv_sem=gate_rs.at[source],
+            device_id=(to, t), device_id_type=MESH,
+        )
+
+    def stat_copy(k, to, source):
+        return pltpu.make_async_remote_copy(
+            src_ref=stat, dst_ref=statall.at[source],
+            send_sem=stat_ss.at[k], recv_sem=stat_rs.at[source],
+            device_id=(to, t), device_id_type=MESH,
+        )
+
+    def num_copy(k, to, source):
+        return pltpu.make_async_remote_copy(
+            src_ref=num, dst_ref=numall.at[source],
+            send_sem=num_ss.at[k], recv_sem=num_rs.at[source],
+            device_id=(to, t), device_id_type=MESH,
+        )
+
+    def forward(held, source, target_batch):
+        return pltpu.make_async_remote_copy(
+            src_ref=held, dst_ref=recv.at[target_batch, source],
+            send_sem=fwd_ss.at[source], recv_sem=fwd_rs.at[source],
+            device_id=(me, other), device_id_type=MESH,
+        )
+
+    def send_tokens(k, carry):
+        tok_copy(k, peer(k), me).start()
+        return carry
+
+    def send_gates(k, carry):
+        gate_copy(k, peer(k), me).start()
+        return carry
+
+    lax.fori_loop(1, per_group, send_tokens, 0)
+    for far in FAR_ORDER[:-1]:
+        lax.fori_loop(far * per_group, (far + 1) * per_group, send_tokens, 0)
+    own_copy = pltpu.make_async_copy(psend.at[me], recv.at[t, me], own_sem)
+    own_copy.start()
+    forward(psend.at[me], me, t).start()
 
     quarter = m // 4
     stacked = jnp.concatenate([gate_ref[...]] * 4, axis=0)
@@ -181,77 +265,7 @@
     for r in range(n):
         gsend[r] = packed[r * quarter : (r + 1) * quarter]
 
-    loads[0].wait()
-    perm = one_hot(col == (row & (m - 1)) * n + (row >> log_m), BF16)
-    for j in range(width // 512):
-        cols = slice(j * 512, (j + 1) * 512)
-        psend[:, :, cols] = dot(perm, tok[t, :, cols]).astype(BF16).reshape(n, m, 512)
-
-    head_of = iota((heads, local), 1) >> log_hd
-    mine = head_of == iota((heads, local), 0)
-    for b in range(seqs):
-        qblk[b * heads : (b + 1) * heads] = jnp.where(
-            mine, query_ref[b : b + 1, :].astype(F32), 0.0
-        ).astype(BF16)
-    scores[...] = jnp.zeros_like(scores)
-
-    pl.semaphore_wait(barrier, n)
-
-    def peer(k):
-        far = lax.div(k, per_group)
-        near = lax.rem(k, per_group)
-        zone = lax.rem(lax.div(me, per_group) + far, GROUPS)
-        return zone * per_group + lax.rem(lax.rem(me, per_group) + near, per_group)
-
-    def tok_copy(k, to, source):
-        return pltpu.make_async_remote_copy(
-            src_ref=psend.at[to], dst_ref=recv.at[t, source],
-            send_sem=tok_ss.at[k], recv_sem=tok_rs.at[source],
-            device_id=(to, t), device_id_type=MESH,
-        )
-
-    def gate_copy(k, to, source):
-        return pltpu.make_async_remote_copy(
-            src_ref=gsend.at[to], dst_ref=grecv.at[source],
-            send_sem=gate_ss.at[k], recv_sem=gate_rs.at[source],
-            device_id=(to, t), device_id_type=MESH,
-        )
-
-    def stat_copy(k, to, source):
-        return pltpu.make_async_remote_copy(
-            src_ref=stat, dst_ref=statall.at[source],
-            send_sem=stat_ss.at[k], recv_sem=stat_rs.at[source],
-            device_id=(to, t), device_id_type=MESH,
-        )
-
-    def num_copy(k, to, source):
-        return pltpu.make_async_remote_copy(
-            src_ref=num, dst_ref=numall.at[source],
-            send_sem=num_ss.at[k], recv_sem=num_rs.at[source],
-            device_id=(to, t), device_id_type=MESH,
-        )
-
-    def forward(held, source, target_batch):
-        return pltpu.make_async_remote_copy(
-            src_ref=held, dst_ref=recv.at[target_batch, source],
-            send_sem=fwd_ss.at[source], recv_sem=fwd_rs.at[source],
-            device_id=(me, other), device_id_type=MESH,
-        )
-
-    def send_tokens(k, carry):
-        tok_copy(k, peer(k), me).start()
-        return carry
-
-    def send_gates(k, carry):
-        gate_copy(k, peer(k), me).start()
-        return carry
-
     lax.fori_loop(1, n, send_gates, 0)
-    for lo, hi in SEND_ORDER(per_group):
-        lax.fori_loop(lo, hi, send_tokens, 0)
-    own_copy = pltpu.make_async_copy(psend.at[me], recv.at[t, me], own_sem)
-    own_copy.start()
-    forward(psend.at[me], me, t).start()
 
     loads[1].wait()
     loads[2].wait()
@@ -309,13 +323,8 @@
     statall[me] = stat[...]
     numall[me] = num[...]
     lax.fori_loop(1, n, send_read, 0)
-
-    def out_copies(zone):
-        rows = pl.ds(pl.multiple_of(zone * per_group * m, per_group * m), per_group * m)
-        return (
-            pltpu.make_async_copy(kst.at[:, rows], kc_ref.at[:, rows], out_sem.at[0, zone]),
-            pltpu.make_async_copy(vst.at[:, rows], vc_ref.at[:, rows], out_sem.at[1, zone]),
-        )
+    last = FAR_ORDER[-1] * per_group
+    lax.fori_loop(last, last + per_group, send_tokens, 0)
 
     def pass_on(far, near_from):
         def step(near, carry):
@@ -347,8 +356,6 @@
             return carry
 
         lax.fori_loop(0, tiles, tile, 0)
-        for copy in out_copies(zone):
-            copy.start()
 
     def finish_gates():
         def arrived(k, carry):
@@ -434,17 +441,13 @@
         return carry
 
     lax.fori_loop(0, n, passed, 0)
-    for zone in range(GROUPS):
-        for copy in out_copies(zone):
-            copy.wait()
 
 
 FAR_ORDER = (1, 3, 2)
 
 
-def SEND_ORDER(per_group):
-    order = [(far * per_group, (far + 1) * per_group) for far in (2, 1, 3)]
-    return order + [(1, per_group)]
+def room(rows, local):
+    return 67043328 - 4 * rows * local - 128 * 1024
 
 
 def body(tokens, key_weight, value_weight, cum_gate, new_input, new_query, new_gate, out_weight):
@@ -456,28 +459,30 @@
     m = span // n
     out_cols = out_weight.shape[1]
     gates = jnp.swapaxes(cum_gate, 1, 2).reshape(seqs * heads, span)
-    anywhere = pl.BlockSpec(memory_space=pl.ANY)
+    far_off = pl.BlockSpec(memory_space=pltpu.HBM)
     inside = pl.BlockSpec(memory_space=pltpu.VMEM)
     dma = pltpu.SemaphoreType.DMA
     key_cache, value_cache, gate_cache, mixed = pl.pallas_call(
         functools.partial(kernel, n, m, heads, head_size),
         out_shape=(
-            jax.ShapeDtypeStruct((seqs, span, local), BF16),
-            jax.ShapeDtypeStruct((seqs, span, local), BF16),
-            jax.ShapeDtypeStruct((seqs * heads, span), F32),
-            jax.ShapeDtypeStruct((seqs, out_cols), BF16),
+            pltpu.VMEM((seqs, span, local), BF16),
+            pltpu.VMEM((seqs, span, local), BF16),
+            pltpu.VMEM((seqs * heads, span), F32),
+            pltpu.VMEM((seqs, out_cols), BF16),
         ),
-        in_specs=[anywhere, anywhere, anywhere, inside, inside, inside, inside, anywhere],
-        out_specs=(anywhere, anywhere, inside, inside),
+        in_specs=[far_off] * 8,
+        out_specs=(inside, inside, inside, inside),
         scratch_shapes=[
+            pltpu.VMEM((seqs * heads, span), F32),
+            pltpu.VMEM(new_input.shape, BF16),
+            pltpu.VMEM(new_query.shape, BF16),
+            pltpu.VMEM(new_gate.shape, F32),
             pltpu.VMEM((seqs, span, width), BF16),
             pltpu.VMEM((width, local), BF16),
             pltpu.VMEM((width, local), BF16),
             pltpu.VMEM(out_weight.shape, BF16),
             pltpu.VMEM((n, m, width), BF16),
             pltpu.VMEM((seqs, n, m, width), BF16),
-            pltpu.VMEM((seqs, span, local), BF16),
-            pltpu.VMEM((seqs, span, local), BF16),
             pltpu.VMEM((n, m // 4, 128), F32),
             pltpu.VMEM((n, m // 4, 128), F32),
             pltpu.VMEM((seqs * heads, local), BF16),
@@ -492,14 +497,13 @@
             pltpu.VMEM((n + 8, 128), F32),
             pltpu.VMEM((seqs, out_cols), BF16),
             pltpu.VMEM((seqs, out_cols), BF16),
-            dma((5,)),
+            dma((9,)),
             dma,
-            dma((2, GROUPS)),
         ]
         + [dma((n,))] * 10
         + [dma, dma],
         compiler_params=pltpu.CompilerParams(
-            collective_id=0, has_side_effects=True, vmem_limit_bytes=60 * 1024 * 1024
+            collective_id=0, has_side_effects=True, vmem_limit_bytes=room(seqs * span, local)
         ),
     )(tokens, key_weight, value_weight, gates, new_input, new_query, new_gate, out_weight)
     gate_cache = jnp.swapaxes(gate_cache.reshape(seqs, heads, span), 1, 2)

time: 52.7 us -> 41.9 us (0.80)
  the two profiles are of different devices: /device:TPU:9 before, /device:TPU:0 now
where the time goes in v2:
time: 41.9 us; the launch traced here: 41.2 us
  Pallas kernels  37.5 us (89%)
  local copies, waits for them, and re-layouts  3.07 us (7%)
  between operations  0.64 us (2%)
    pallas_call x1, Pallas kernels, body(): pl.pallas_call(functools.partial(kernel, n, m, heads, head_size), out_sha...  37.5 us
    unnamed x4, local copies, waits for them, and re-layouts  3.07 us

profile of v2, /device:TPU:0, one launch (start us, length us, event | category | flops | bytes accessed | tf_op | source)
XLA Modules:
  0.0 41.2 jit_solution(9620714818325427459)
XLA Ops:
  0.6 37.5 %shard_map.111 = (bf16[2,256,1024]{2,1,0:T(8,128)(2,1)S(1)}, bf16[2,256,1024]{2,1,0:T(8,128)(2,1)S(1)}, f32[32,256]{1,0:T(8,128)S(1)}, bf16[2,128]{1,0:T(2,128)(2,1)S(1)}) custom-call(bf16[2,256,2048]{2,1,0:T(8,128)(2,1)} %tokens_ref.1, bf16[2048,1024]{1,0:T(8,128)(2,1)} %wk_ref.1, bf16[2048,1024]{1,0:T(8,128)(2,1)} %wv_ref.1, f32[32,256]{1,0:T(8,128)} %bitcast.17, ...), custom_call_target="tpu_custom_call" | custom-call | tf_op jit(solution)/shard_map/pallas_call | solution.py:465
  38.2 1.0 %copy.18 = bf16[2,1,256,1024]{3,2,1,0:T(8,128)(2,1)} copy(bf16[2,1,256,1024]{3,2,1,0:T(8,128)(2,1)S(1)} %bitcast.15) | data formatting | bytes 2097152
  39.1 1.0 %copy.19 = bf16[2,1,256,1024]{3,2,1,0:T(8,128)(2,1)} copy(bf16[2,1,256,1024]{3,2,1,0:T(8,128)(2,1)S(1)} %bitcast.14) | data formatting | bytes 2097152
  40.1 0.5 %copy.21 = bf16[2,128]{1,0:T(2,128)(2,1)} copy(bf16[2,128]{1,0:T(2,128)(2,1)S(1)} %get-tuple-element.19) | data formatting | bytes 1024
  40.6 0.6 %copy.20 = f32[2,1,256,16]{2,3,1,0:T(8,128)} copy(f32[2,1,256,16]{2,3,1,0:T(8,128)S(1)} %bitcast.16) | data formatting | bytes 65536
